TPU v7x, 32 devices: a whole 2x2x4 slice. The times are simulated.
32 devices in a mesh: kv: 4 (over y, x), tp: 8 (over z, core).
Axes of the slice: x: 2, y: 2, z: 4, core: 2. Of those that a mesh axis runs over, the one named last changes fastest.
Arguments:
- tokens: bfloat16 [384, 4096], P('kv', 'tp'), may hold values from -20 to 20
- state: float32 [384, 32, 4096], P('kv', 'tp'), may hold values from -4 to 4
- w_query: bfloat16 [4096, 2048], P(None, 'tp'), may hold values from -0.09375 to 0.09375
- w_key: bfloat16 [4096, 2048], P(None, 'tp'), may hold values from -0.09375 to 0.09375
- w_value: bfloat16 [4096, 2048], P(None, 'tp'), may hold values from -0.09375 to 0.09375
- w_gate: bfloat16 [4096, 2048], P(None, 'tp'), may hold values from -0.09375 to 0.09375
- w_decay: bfloat16 [4096, 32], replicated, may hold values from -0.09375 to 0.09375
- w_beta: bfloat16 [4096, 32], replicated, may hold values from -0.09375 to 0.09375
- decay_rate: float32 [32], P('tp'), may hold values from 0.03 to 3
- decay_bias: float32 [32], P('tp'), may hold values from -1 to 1
- mix_gain: float32 [4096], replicated, may hold values from 0.1 to 1.9
- out_gain: float32 [64], replicated, may hold values from 0.1 to 1.9
- w_out: bfloat16 [2048, 4096], P('tp'), may hold values from -0.125 to 0.125
- ffn_gain: float32 [4096], replicated, may hold values from 0.1 to 1.9
- w_up: bfloat16 [4096, 16384], P('tp', 'kv'), may hold values from -0.09375 to 0.09375
- w_down: bfloat16 [16384, 4096], P('kv', 'tp'), may hold values from -0.046875 to 0.046875
Outputs:
- mixed: bfloat16 [384, 4096], P('kv', 'tp')
- new_state: float32 [384, 32, 4096], P('kv', 'tp')
All inputs are finite; a program needn't handle non-finite values.
Results may differ from a plain program's by a relative error of at most 0.024.
Values may be sent and summed in bfloat16 or wider, within the bound.
A program may use at most 128 MiB of HBM per device.

v0:
```python
import jax
import jax.numpy as jnp
from jax import lax
from jax.sharding import PartitionSpec as P

D = 4096
HEAD_DIM = 64
EPS = 1e-06


def unit_norm(vector):
    return vector * lax.rsqrt(jnp.sum(vector * vector, axis=-1, keepdims=True) + EPS)


def local(
    tokens,
    state,
    w_query,
    w_key,
    w_value,
    w_gate,
    w_decay,
    w_beta,
    decay_rate,
    decay_bias,
    mix_gain,
    out_gain,
    w_out,
    ffn_gain,
    w_up,
    w_down,
):
    rows = tokens.shape[0]
    width_share = tokens.shape[1]
    head_count = w_query.shape[1] // HEAD_DIM
    full_rows = lax.all_gather(tokens, "tp", axis=1, tiled=True)
    full_f = full_rows.astype(jnp.float32)
    normed = (
        full_f * lax.rsqrt(jnp.mean(full_f * full_f, axis=-1, keepdims=True) + EPS) * mix_gain
    ).astype(jnp.bfloat16)
    query = jnp.dot(normed, w_query, preferred_element_type=jnp.float32).reshape(
        rows, head_count, HEAD_DIM
    )
    key_proj = jnp.dot(normed, w_key, preferred_element_type=jnp.float32).reshape(
        rows, head_count, HEAD_DIM
    )
    value = jnp.dot(normed, w_value, preferred_element_type=jnp.float32).reshape(
        rows, head_count, HEAD_DIM
    )
    gate = jnp.dot(normed, w_gate, preferred_element_type=jnp.float32).reshape(
        rows, head_count, HEAD_DIM
    )
    query = unit_norm(query) * HEAD_DIM ** (-0.5)
    key_proj = unit_norm(key_proj)
    head_start = lax.axis_index("tp") * head_count
    decay_cols = lax.dynamic_slice_in_dim(w_decay, head_start, head_count, 1)
    beta_cols = lax.dynamic_slice_in_dim(w_beta, head_start, head_count, 1)
    pre_decay = jnp.dot(normed, decay_cols, preferred_element_type=jnp.float32)
    decay = jnp.exp(-decay_rate * jax.nn.softplus(pre_decay + decay_bias))
    strength = jax.nn.sigmoid(jnp.dot(normed, beta_cols, preferred_element_type=jnp.float32))
    matrix = state.reshape(rows, head_count, HEAD_DIM, HEAD_DIM) * decay[:, :, None, None]
    recalled = jnp.einsum("bhk,bhkv->bhv", key_proj, matrix, precision=lax.Precision.HIGHEST)
    delta = (value - recalled) * strength[:, :, None]
    matrix = matrix + key_proj[:, :, :, None] * delta[:, :, None, :]
    head_out = jnp.einsum("bhk,bhkv->bhv", query, matrix, precision=lax.Precision.HIGHEST)
    head_out = (
        head_out
        * lax.rsqrt(jnp.mean(head_out * head_out, axis=-1, keepdims=True) + EPS)
        * out_gain
        * jax.nn.silu(gate)
    )
    head_out = head_out.reshape(rows, head_count * HEAD_DIM).astype(jnp.bfloat16)
    partial_value = jnp.dot(head_out, w_out, preferred_element_type=jnp.float32)
    feature_start = lax.axis_index("tp") * width_share
    gain_share = lax.dynamic_slice_in_dim(ffn_gain, feature_start, width_share, 0)
    resid = tokens.astype(jnp.float32) + lax.psum_scatter(
        partial_value.astype(jnp.bfloat16), "tp", scatter_dimension=1, tiled=True
    ).astype(jnp.float32)
    squares = lax.psum(jnp.sum(resid * resid, axis=-1), "tp")
    scale = lax.rsqrt(squares[:, None] / D + EPS)
    ffn_in = (resid * scale * gain_share).astype(jnp.bfloat16)
    up_part = jnp.dot(
        lax.all_gather(ffn_in, "kv", axis=0, tiled=True), w_up, preferred_element_type=jnp.float32
    )
    up_full = lax.psum(up_part.astype(jnp.bfloat16), "tp").astype(jnp.float32)
    hidden = jnp.square(jax.nn.relu(up_full)).astype(jnp.bfloat16)
    down = lax.psum_scatter(
        jnp.dot(hidden, w_down, preferred_element_type=jnp.float32).astype(jnp.bfloat16),
        "kv",
        scatter_dimension=0,
        tiled=True,
    ).astype(jnp.float32)
    mixed = (resid + down).astype(jnp.bfloat16)
    return (mixed, matrix.reshape(rows, head_count, HEAD_DIM * HEAD_DIM))


def solution(mesh):
    in_specs = (
        P("kv", "tp"),
        P("kv", "tp", None),
        P(None, "tp"),
        P(None, "tp"),
        P(None, "tp"),
        P(None, "tp"),
        P(),
        P(),
        P("tp"),
        P("tp"),
        P(),
        P(),
        P("tp", None),
        P(),
        P("tp", "kv"),
        P("kv", "tp"),
    )
    out_specs = (P("kv", "tp"), P("kv", "tp", None))
    return jax.shard_map(local, mesh=mesh, in_specs=in_specs, out_specs=out_specs, check_vma=False)
```

profile of v0, /device:TPU:0, one launch (start us, length us, event | category | flops | bytes accessed | tf_op | source)
XLA Modules:
  0.0 233.8 jit_solution(16335360079471447695)
XLA Ops:
  7.2 0.0 copy-start
  7.2 0.0 reduce-scatter.3.cloned.1.call-start
  7.2 0.8 neg.14
  8.0 17.4 %all_gather.6 = bf16[96,4096]{1,0:T(8,128)(2,1)S(1)} all-gather(bf16[96,512]{1,0:T(8,128)(2,1)} %param.16), channel_id=1, replica_groups=mesh['kv'=4,'tp'=8] {'tp'}, dimensions={1}, use_global_device_ids=true | all-gather | bytes 884736 | tf_op jit(solution)/shard_map/all_gather | solution.py:36
  25.4 0.0 copy-start.6
  25.4 0.0 copy-start.9
  25.4 0.3 fusion.2
  25.7 2.7 %fusion.21 = f32[96,256]{0,1:T(8,128)S(1)} fusion(bf16[4096,256]{1,0:T(8,128)(2,1)} %param.20, bf16[96,4096]{1,0:T(8,128)(2,1)S(1)} %all_gather.6, f32[4096]{0:T(1024)} %param.26, f32[96]{0:T(128)S(1)} %add_rsqrt_fusion.4), kind=kOutput, calls=%fused_computation.45 | convolution fusion | flops 202899456 | bytes 2998656 | tf_op jit(solution)/shard_map/dot_general | solution.py:47
  28.4 0.0 copy-done.6
  28.4 0.0 copy-done.9
  28.4 0.0 copy-start.7
  28.5 1.0 fusion.18
  29.5 0.6 copy-done.7
  30.0 0.0 copy-start.8
  30.0 1.0 multiply_reduce_fusion.4
  31.1 0.6 copy-done.8
  31.6 1.0 multiply_reduce_fusion.5
  32.7 0.0 copy-start.10
  32.7 9.2 %copy.22 = f32[96,4,4096]{0,2,1:T(8,128)} copy(f32[96,4,4096]{2,1,0:T(4,128)} %param.17) | data formatting | bytes 12582912 | tf_op args[1]
  41.9 1.2 fusion.8
  43.1 0.0 copy-done.10
  43.1 1.2 fusion.12
  44.4 0.0 copy-start.2
  44.4 5.0 %multiply_reduce_fusion.1 = f32[96,4,64]{0,2,1:T(8,128)S(1)} fusion(f32[96,4,64,64]{0,3,2,1:T(8,128)} %bitcast.21, f32[96,4,64]{0,2,1:T(8,128)S(1)} %broadcast_multiply_fusion.1, f32[96,4]{0,1:T(4,128)S(1)} %fusion.12), kind=kLoop, calls=%fused_computation.2 | loop fusion | flops 4694016 | bytes 6489600 | tf_op jit(solution)/shard_map/bhk,bhkv->bhv/dot_general | solution.py:62
  49.5 0.7 copy-done.2
  50.2 0.0 copy-start.5
  50.2 4.2 %broadcast_multiply_fusion = (f32[96,4,64,64]{0,3,2,1:T(8,128)}, f32[96,4,64]{0,2,1:T(8,128)S(1)}) fusion(f32[96,4,64]{0,2,1:T(8,128)S(1)} %get-tuple-element.10, f32[96,4,64]{0,2,1:T(8,128)S(1)} %broadcast_multiply_fusion.1, f32[96,4,64,64]{0,3,2,1:T(8,128)S(1)} %bitcast.22, f32[96,4]{0,1:T(4,128)S(1)} %fusion.12, f32[96,4,64]{0,2,1:T(8,128)S(1)} %get-tuple-element.11), kind=kLoop, calls=%fused_computation.6 | loop fusion | flops 7839744 | bytes 12977664 | tf_op jit(solution)/shard_map/mul | solution.py:64
  54.4 0.0 copy-start.3
  54.4 0.0 copy-done.5
  54.4 0.1 multiply_convert_fusion.5
  54.5 0.0 copy-done
  54.5 1.4 convolution_convert_fusion.1
  55.9 0.0 reduce-scatter.3.cloned.1.call-update
  55.9 0.0 all-reduce.2.cloned.1.call-start
  56.0 0.8 dynamic_slice.11
  56.7 32.4 %reduce-scatter.3.cloned.1.call-done = bf16[96,512]{1,0:T(8,128)(2,1)} async-done(((bf16[96,4096]{1,0:T(8,128)(2,1)}), bf16[96,512]{1,0:T(8,128)(2,1)}) %reduce-scatter.3.cloned.1.call-update) | async-done | bytes 98320 | tf_op jit(solution)/shard_map/reduce_scatter | solution.py:76
  89.2 0.0 copy-done.3
  89.2 1.0 multiply_reduce_fusion.2
  90.2 13.8 %psum.14 = f32[96]{0:T(128)S(1)} all-reduce(f32[96]{0:T(128)S(1)} %multiply_reduce_fusion.2), channel_id=1, replica_groups=mesh['kv'=4,'tp'=8] {'tp'}, use_global_device_ids=true, to_apply=%region_6.7 | all-reduce | flops 96 | bytes 768 | tf_op jit(solution)/shard_map/psum | solution.py:79
  104.0 1.0 multiply_convert_fusion.4
  105.0 10.1 %all_gather.7 = bf16[384,512]{1,0:T(8,128)(2,1)S(1)} all-gather(bf16[96,512]{1,0:T(8,128)(2,1)S(1)} %multiply_convert_fusion.4), channel_id=1, replica_groups=mesh['kv'=4,'tp'=8] {'kv'}, dimensions={0}, use_global_device_ids=true | all-gather | bytes 491520 | tf_op jit(solution)/shard_map/all_gather | solution.py:83
  115.0 5.7 %convolution_convert_fusion = bf16[384,4096]{1,0:T(8,128)(2,1)} fusion(bf16[384,512]{1,0:T(8,128)(2,1)S(1)} %all_gather.7, bf16[512,4096]{1,0:T(8,128)(2,1)} %param.30), kind=kOutput, calls=%fused_computation.4 | convolution fusion | flops 1612185600 | bytes 7733248 | tf_op jit(solution)/shard_map/dot_general | solution.py:82
  120.7 0.0 all-reduce.2.cloned.1.call-update
  120.7 0.2 reduce-scatter.5.cloned.1.call-start
  120.9 74.3 %all-reduce.2.cloned.1.call-done = bf16[384,4096]{1,0:T(8,128)(2,1)} async-done(((bf16[384,4096]{1,0:T(8,128)(2,1)}), bf16[384,4096]{1,0:T(8,128)(2,1)}) %all-reduce.2.cloned.1.call-update) | async-done | bytes 3145744 | tf_op jit(solution)/shard_map/psum | solution.py:85
  195.2 5.7 %fusion.5 = bf16[384,512]{1,0:T(8,128)(2,1)} fusion(bf16[4096,512]{1,0:T(8,128)(2,1)} %param.31, bf16[384,4096]{1,0:T(8,128)(2,1)} %all-reduce.2.cloned.1.call-done), kind=kOutput, calls=%fused_computation.14 | convolution fusion | flops 1617100800 | bytes 7733248 | tf_op jit(solution)/shard_map/dot_general | solution.py:88
  200.9 0.0 reduce-scatter.5.cloned.1.call-update
  200.9 9.8 %bitcast_add_fusion = f32[96,4,4096]{0,2,1:T(8,128)} fusion(f32[96,4,64,64]{0,3,2,1:T(8,128)} %get-tuple-element.4, f32[96,4,4096]{0,2,1:T(8,128)} %copy.22, f32[96,4]{0,1:T(4,128)S(1)} %fusion.12), kind=kLoop, calls=%fused_computation | loop fusion | flops 3145728 | bytes 18875904 | tf_op jit(solution)/shard_map/add | solution.py:64
  210.7 0.0 copy-start.4
  210.7 0.0 copy-start.1
  210.7 9.6 %copy.27 = f32[96,4,4096]{2,1,0:T(4,128)} copy(f32[96,4,4096]{0,2,1:T(8,128)} %bitcast_add_fusion) | data formatting | bytes 12582912
  220.3 5.4 %reduce-scatter.5.cloned.1.call-done = bf16[96,512]{1,0:T(8,128)(2,1)} async-done(((bf16[384,512]{1,0:T(8,128)(2,1)}), bf16[96,512]{1,0:T(8,128)(2,1)}) %reduce-scatter.5.cloned.1.call-update) | async-done | bytes 98320 | tf_op jit(solution)/shard_map/reduce_scatter | solution.py:87
  225.7 0.0 copy-done.4
  225.7 1.6 add_convert_fusion
  227.3 0.0 copy-done.1
  (8 shorter events, 0.1 us)
Async XLA Ops:
  7.2 47.3 %copy-start = (bf16[256,4096]{1,0:T(8,128)(2,1)S(1)}, bf16[256,4096]{1,0:T(8,128)(2,1)}, u32[]{:S(2)}) copy-start(bf16[256,4096]{1,0:T(8,128)(2,1)} %param.28) | copy-start | bytes 6291460
  7.2 82.0 %reduce-scatter.3.cloned.1.call-start = ((), (), s32[]{:S(2)}) async-start(), calls=%async_computation.2 | async-start | bytes 884736 | tf_op jit(solution)/shard_map/reduce_scatter | solution.py:76
  25.4 3.0 %copy-start.6 = (bf16[4096,256]{1,0:T(8,128)(2,1)S(1)}, bf16[4096,256]{1,0:T(8,128)(2,1)}, u32[]{:S(2)}) copy-start(bf16[4096,256]{1,0:T(8,128)(2,1)} %param.21) | copy-start | bytes 6291460
  25.4 3.0 %copy-start.9 = (f32[4096]{0:T(1024)S(1)}, f32[4096]{0:T(1024)}, u32[]{:S(2)}) copy-start(f32[4096]{0:T(1024)} %param.26) | copy-start | bytes 49156
  28.4 1.6 copy-start.7
  30.0 1.6 copy-start.8
  32.7 10.4 %copy-start.10 = (f32[4]{0:T(128)S(1)}, f32[4]{0:T(128)}, u32[]{:S(2)}) copy-start(f32[4]{0:T(128)} %param.25) | copy-start | bytes 52
  44.4 5.8 %copy-start.2 = (f32[96,4,4096]{0,2,1:T(8,128)S(1)}, f32[96,4,4096]{0,2,1:T(8,128)}, u32[]{:S(2)}) copy-start(f32[96,4,4096]{0,2,1:T(8,128)} %copy.22) | copy-start | bytes 18874372
  50.2 4.2 %copy-start.5 = (f32[64]{0:T(128)S(1)}, f32[64]{0:T(128)}, u32[]{:S(2)}) copy-start(f32[64]{0:T(128)} %param.27) | copy-start | bytes 772
  54.4 34.8 %copy-start.3 = (bf16[96,512]{1,0:T(8,128)(2,1)S(1)}, bf16[96,512]{1,0:T(8,128)(2,1)}, u32[]{:S(2)}) copy-start(bf16[96,512]{1,0:T(8,128)(2,1)} %param.16) | copy-start | bytes 294916
  55.9 139.3 %all-reduce.2.cloned.1.call-start = ((), (), s32[]{:S(2)}) async-start(), calls=%async_computation.3 | async-start | bytes 6291456 | tf_op jit(solution)/shard_map/psum | solution.py:85
  120.7 105.0 %reduce-scatter.5.cloned.1.call-start = ((), (), s32[]{:S(2)}) async-start(), calls=%async_computation.4 | async-start | bytes 491520 | tf_op jit(solution)/shard_map/reduce_scatter | solution.py:87
  210.7 15.0 %copy-start.4 = (bf16[96,512]{1,0:T(8,128)(2,1)S(1)}, bf16[96,512]{1,0:T(8,128)(2,1)}, u32[]{:S(2)}) copy-start(bf16[96,512]{1,0:T(8,128)(2,1)} %reduce-scatter.3.cloned.1.call-done) | copy-start | bytes 294916
  210.7 16.5 %copy-start.1 = (bf16[256,4096]{1,0:T(8,128)(2,1)S(1)}, bf16[256,4096]{1,0:T(8,128)(2,1)}, u32[]{:S(2)}) copy-start(bf16[256,4096]{1,0:T(8,128)(2,1)} %param.28) | copy-start | bytes 6291460
Sparse Core Ops, SparseCore 0:
  56.0 33.0 reduce-scatter.2
  120.8 74.3 all-reduce.1
  201.1 24.6 reduce-scatter.4
where the time goes:
time: 235 us; the launch traced here: 234 us
  waiting for transfers between devices  112 us (48%)
  blocking collectives  41.3 us (18%)
  other arithmetic  23.9 us (10%)
  local copies, waits for them, and re-layouts  21.4 us (9%)
  matrix products  20.9 us (9%)
  between operations  13.9 us (6%)
    psum x1, waiting for transfers between devices, local(): up_full = lax.psum(up_part.astype(jnp.bfloat16), 'tp').astype(jnp.float32)  74.3 us
    reduce_scatter x1, waiting for transfers between devices, local(): lax.psum_scatter(partial_value.astype(jnp.bfloat16), 'tp', scatter_dimens...  32.4 us
    unnamed x24, local copies, waits for them, and re-layouts  20.7 us
    all_gather x1, blocking collectives, local(): full_rows = lax.all_gather(tokens, 'tp', axis=1, tiled=True)  17.4 us
    psum x1, blocking collectives, local(): squares = lax.psum(jnp.sum(resid * resid, axis=-1), 'tp')  13.8 us
    all_gather x1, blocking collectives, local(): lax.all_gather(ffn_in, 'kv', axis=0, tiled=True)  10.1 us
    add x1, other arithmetic, local(): matrix = matrix + key_proj[:, :, :, None] * delta[:, :, None, :]  9.81 us
    dot_general x1, matrix products, local(): jnp.dot(hidden, w_down, preferred_element_type=jnp.float32)  5.68 us
  transfers between devices with their start and end apart: 3, of which 3 were waited for; matrix products, arithmetic and copies ran while one was open for 9% of the time, Pallas kernels for 0%

commit v1 on v0

--- a/solution.py
+++ b/solution.py
@@ -6,6 +6,11 @@
 D = 4096
 HEAD_DIM = 64
 EPS = 1e-06
+
+
+def summed_here(x, mesh_axis):
+    parts = lax.all_gather(x, mesh_axis)
+    return jnp.sum(parts, axis=0)
 
 
 def unit_norm(vector):
@@ -82,7 +87,7 @@
     up_part = jnp.dot(
         lax.all_gather(ffn_in, "kv", axis=0, tiled=True), w_up, preferred_element_type=jnp.float32
     )
-    up_full = lax.psum(up_part.astype(jnp.bfloat16), "tp").astype(jnp.float32)
+    up_full = summed_here(up_part.astype(jnp.bfloat16), "tp").astype(jnp.float32)
     hidden = jnp.square(jax.nn.relu(up_full)).astype(jnp.bfloat16)
     down = lax.psum_scatter(
         jnp.dot(hidden, w_down, preferred_element_type=jnp.float32).astype(jnp.bfloat16),

time: 235 us -> 391 us (1.66)
  waiting for transfers between devices: 112 us -> 254 us
  other arithmetic: 23.9 us -> 39.1 us
    all_gather x0 -> x1, waiting for transfers between devices: none -> 218 us  [summed_here(): parts = lax.all_gather(x, mesh_axis)]
    psum x1 -> x0, waiting for transfers between devices: 74.3 us -> none  [local(): up_full = lax.psum(up_part.astype(jnp.bfloat16), 'tp').astype(jnp.float32)]
    reduce_sum x0 -> x1, other arithmetic: none -> 15.2 us  [summed_here(): return jnp.sum(parts, axis=0)]
  transfers between devices with their start and end apart: 3 -> 3, of which waited for: 3 -> 3; matrix products, arithmetic and copies ran while one was open for 9% -> 5% of each run, Pallas kernels for 0% -> 0%
where the time goes in v1:
time: 391 us; the launch traced here: 390 us
  waiting for transfers between devices  254 us (65%)
  blocking collectives  41.2 us (11%)
  other arithmetic  39.1 us (10%)
  local copies, waits for them, and re-layouts  21.4 us (5%)
  matrix products  20.9 us (5%)
  between operations  13.9 us (4%)
    all_gather x1, waiting for transfers between devices, summed_here(): parts = lax.all_gather(x, mesh_axis)  218 us
    reduce_scatter x1, waiting for transfers between devices, local(): lax.psum_scatter(partial_value.astype(jnp.bfloat16), 'tp', scatter_dimens...  32.4 us
    unnamed x24, local copies, waits for them, and re-layouts  20.6 us
    all_gather x1, blocking collectives, local(): full_rows = lax.all_gather(tokens, 'tp', axis=1, tiled=True)  17.4 us
    reduce_sum x1, other arithmetic, summed_here(): return jnp.sum(parts, axis=0)  15.2 us
    psum x1, blocking collectives, local(): squares = lax.psum(jnp.sum(resid * resid, axis=-1), 'tp')  13.8 us
    all_gather x1, blocking collectives, local(): lax.all_gather(ffn_in, 'kv', axis=0, tiled=True)  9.97 us
    add x1, other arithmetic, local(): matrix = matrix + key_proj[:, :, :, None] * delta[:, :, None, :]  9.87 us
  transfers between devices with their start and end apart: 3, of which 3 were waited for; matrix products, arithmetic and copies ran while one was open for 5% of the time, Pallas kernels for 0%

profile of v1, /device:TPU:0, one launch (start us, length us, event | category | flops | bytes accessed | tf_op | source)
XLA Modules:
  0.0 390.5 jit_solution(9699485979794289456)
XLA Ops:
  7.2 0.0 copy-start
  7.2 0.0 reduce-scatter.3.cloned.1.call-start
  7.2 0.8 neg.14
  8.0 17.4 %all_gather.12 = bf16[96,4096]{1,0:T(8,128)(2,1)S(1)} all-gather(bf16[96,512]{1,0:T(8,128)(2,1)} %param.16), channel_id=1, replica_groups=mesh['kv'=4,'tp'=8] {'tp'}, dimensions={1}, use_global_device_ids=true | all-gather | bytes 884736 | tf_op jit(solution)/shard_map/all_gather | solution.py:41
  25.4 0.0 copy-start.6
  25.4 0.0 copy-start.9
  25.4 0.3 fusion.2
  25.7 2.7 fusion.21
  28.4 0.0 copy-done.6
  28.4 0.0 copy-done.9
  28.4 0.0 copy-start.7
  28.5 1.0 fusion.18
  29.5 0.6 copy-done.7
  30.0 0.0 copy-start.8
  30.0 1.0 multiply_reduce_fusion.4
  31.1 0.6 copy-done.8
  31.6 1.0 multiply_reduce_fusion.5
  32.7 0.0 copy-start.10
  32.7 9.1 %copy.22 = f32[96,4,4096]{0,2,1:T(8,128)} copy(f32[96,4,4096]{2,1,0:T(4,128)} %param.17) | data formatting | bytes 12582912 | tf_op args[1]
  41.8 1.2 fusion.8
  43.1 0.0 copy-done.10
  43.1 1.2 fusion.12
  44.3 0.0 copy-start.2
  44.4 5.0 %multiply_reduce_fusion.1 = f32[96,4,64]{0,2,1:T(8,128)S(1)} fusion(f32[96,4,64,64]{0,3,2,1:T(8,128)} %bitcast.22, f32[96,4,64]{0,2,1:T(8,128)S(1)} %broadcast_multiply_fusion.1, f32[96,4]{0,1:T(4,128)S(1)} %fusion.12), kind=kLoop, calls=%fused_computation.2 | loop fusion | flops 4694016 | bytes 6489600 | tf_op jit(solution)/shard_map/bhk,bhkv->bhv/dot_general | solution.py:67
  49.4 0.7 copy-done.2
  50.1 0.0 copy-start.5
  50.1 4.2 %broadcast_multiply_fusion = (f32[96,4,64,64]{0,3,2,1:T(8,128)}, f32[96,4,64]{0,2,1:T(8,128)S(1)}) fusion(f32[96,4,64]{0,2,1:T(8,128)S(1)} %get-tuple-element.10, f32[96,4,64]{0,2,1:T(8,128)S(1)} %broadcast_multiply_fusion.1, f32[96,4,64,64]{0,3,2,1:T(8,128)S(1)} %bitcast.23, f32[96,4]{0,1:T(4,128)S(1)} %fusion.12, f32[96,4,64]{0,2,1:T(8,128)S(1)} %get-tuple-element.11), kind=kLoop, calls=%fused_computation.6 | loop fusion | flops 7839744 | bytes 12977664 | tf_op jit(solution)/shard_map/mul | solution.py:69
  54.3 0.0 copy-start.3
  54.4 0.0 copy-done.5
  54.4 0.1 multiply_convert_fusion.5
  54.5 0.0 copy-done
  54.5 1.4 convolution_convert_fusion.1
  55.9 0.0 reduce-scatter.3.cloned.1.call-update
  55.9 0.0 all-gather.3.cloned.1.call-start
  55.9 0.8 dynamic_slice.11
  56.7 32.4 %reduce-scatter.3.cloned.1.call-done = bf16[96,512]{1,0:T(8,128)(2,1)} async-done(((bf16[96,4096]{1,0:T(8,128)(2,1)}), bf16[96,512]{1,0:T(8,128)(2,1)}) %reduce-scatter.3.cloned.1.call-update) | async-done | bytes 98320 | tf_op jit(solution)/shard_map/reduce_scatter | solution.py:81
  89.1 0.0 copy-done.3
  89.1 1.0 multiply_reduce_fusion.2
  90.1 13.8 %psum.7 = f32[96]{0:T(128)S(1)} all-reduce(f32[96]{0:T(128)S(1)} %multiply_reduce_fusion.2), channel_id=1, replica_groups=mesh['kv'=4,'tp'=8] {'tp'}, use_global_device_ids=true, to_apply=%region_6.7 | all-reduce | flops 96 | bytes 768 | tf_op jit(solution)/shard_map/psum | solution.py:84
  103.9 1.0 multiply_convert_fusion.4
  104.9 10.0 %all_gather.13 = bf16[384,512]{1,0:T(8,128)(2,1)S(1)} all-gather(bf16[96,512]{1,0:T(8,128)(2,1)S(1)} %multiply_convert_fusion.4), channel_id=1, replica_groups=mesh['kv'=4,'tp'=8] {'kv'}, dimensions={0}, use_global_device_ids=true | all-gather | bytes 491520 | tf_op jit(solution)/shard_map/all_gather | solution.py:88
  114.9 5.7 %convolution_convert_fusion = bf16[384,4096]{1,0:T(8,128)(2,1)} fusion(bf16[384,512]{1,0:T(8,128)(2,1)S(1)} %all_gather.13, bf16[512,4096]{1,0:T(8,128)(2,1)} %param.30), kind=kOutput, calls=%fused_computation.4 | convolution fusion | flops 1612185600 | bytes 7733248 | tf_op jit(solution)/shard_map/dot_general | solution.py:87
  120.5 0.0 all-gather.3.cloned.1.call-update
  120.6 0.2 reduce-scatter.5.cloned.1.call-start
  120.8 217.6 %all-gather.3.cloned.1.call-done = bf16[3072,4096]{1,0:T(8,128)(2,1)} async-done(((bf16[384,4096]{1,0:T(8,128)(2,1)}), bf16[3072,4096]{1,0:T(8,128)(2,1)}) %all-gather.3.cloned.1.call-update) | async-done | bytes 25165840 | tf_op jit(solution)/shard_map/all_gather | solution.py:12
  338.4 15.2 %reduce_sum.62 = bf16[384,4096]{1,0:T(8,128)(2,1)} reduce(bf16[8,384,4096]{2,1,0:T(8,128)(2,1)} %bitcast.24, bf16[]{:T(256)} %constant.37.clone.1), dimensions={0}, to_apply=%region_7.8 | reduce | flops 11010048 | bytes 28311554 | tf_op jit(solution)/shard_map/reduce_sum | solution.py:13
  353.6 5.7 %fusion.5 = bf16[384,512]{1,0:T(8,128)(2,1)} fusion(bf16[4096,512]{1,0:T(8,128)(2,1)} %param.31, bf16[384,4096]{1,0:T(8,128)(2,1)} %reduce_sum.62), kind=kOutput, calls=%fused_computation.14 | convolution fusion | flops 1617100800 | bytes 7733248 | tf_op jit(solution)/shard_map/dot_general | solution.py:93
  359.3 0.0 reduce-scatter.5.cloned.1.call-update
  359.3 9.9 %bitcast_add_fusion = f32[96,4,4096]{0,2,1:T(8,128)} fusion(f32[96,4,64,64]{0,3,2,1:T(8,128)} %get-tuple-element.4, f32[96,4,4096]{0,2,1:T(8,128)} %copy.22, f32[96,4]{0,1:T(4,128)S(1)} %fusion.12), kind=kLoop, calls=%fused_computation | loop fusion | flops 3145728 | bytes 18875904 | tf_op jit(solution)/shard_map/add | solution.py:69
  369.2 0.0 copy-start.4
  369.2 0.0 copy-start.1
  369.2 9.6 %copy.27 = f32[96,4,4096]{2,1,0:T(4,128)} copy(f32[96,4,4096]{0,2,1:T(8,128)} %bitcast_add_fusion) | data formatting | bytes 12582912
  378.7 3.6 reduce-scatter.5.cloned.1.call-done
  382.4 0.0 copy-done.4
  382.4 1.6 add_convert_fusion
  383.9 0.0 copy-done.1
  (8 shorter events, 0.1 us)
Async XLA Ops:
  7.2 47.3 %copy-start = (bf16[256,4096]{1,0:T(8,128)(2,1)S(1)}, bf16[256,4096]{1,0:T(8,128)(2,1)}, u32[]{:S(2)}) copy-start(bf16[256,4096]{1,0:T(8,128)(2,1)} %param.28) | copy-start | bytes 6291460
  7.2 81.9 %reduce-scatter.3.cloned.1.call-start = ((), (), s32[]{:S(2)}) async-start(), calls=%async_computation.2 | async-start | bytes 884736 | tf_op jit(solution)/shard_map/reduce_scatter | solution.py:81
  25.4 3.0 copy-start.6
  25.4 3.0 copy-start.9
  28.4 1.6 copy-start.7
  30.0 1.6 copy-start.8
  32.7 10.4 %copy-start.10 = (f32[4]{0:T(128)S(1)}, f32[4]{0:T(128)}, u32[]{:S(2)}) copy-start(f32[4]{0:T(128)} %param.25) | copy-start | bytes 52
  44.3 5.8 %copy-start.2 = (f32[96,4,4096]{0,2,1:T(8,128)S(1)}, f32[96,4,4096]{0,2,1:T(8,128)}, u32[]{:S(2)}) copy-start(f32[96,4,4096]{0,2,1:T(8,128)} %copy.22) | copy-start | bytes 18874372
  50.1 4.2 %copy-start.5 = (f32[64]{0:T(128)S(1)}, f32[64]{0:T(128)}, u32[]{:S(2)}) copy-start(f32[64]{0:T(128)} %param.27) | copy-start | bytes 772
  54.3 34.8 %copy-start.3 = (bf16[96,512]{1,0:T(8,128)(2,1)S(1)}, bf16[96,512]{1,0:T(8,128)(2,1)}, u32[]{:S(2)}) copy-start(bf16[96,512]{1,0:T(8,128)(2,1)} %param.16) | copy-start | bytes 294916
  55.9 282.5 %all-gather.3.cloned.1.call-start = ((), (), s32[]{:S(2)}) async-start(), calls=%async_computation.4 | async-start | bytes 28311552 | tf_op jit(solution)/shard_map/all_gather | solution.py:12
  120.6 261.8 %reduce-scatter.5.cloned.1.call-start = ((), (), s32[]{:S(2)}) async-start(), calls=%async_computation.3 | async-start | bytes 491520 | tf_op jit(solution)/shard_map/reduce_scatter | solution.py:92
  369.2 13.2 %copy-start.4 = (bf16[96,512]{1,0:T(8,128)(2,1)S(1)}, bf16[96,512]{1,0:T(8,128)(2,1)}, u32[]{:S(2)}) copy-start(bf16[96,512]{1,0:T(8,128)(2,1)} %reduce-scatter.3.cloned.1.call-done) | copy-start | bytes 294916
  369.2 14.8 %copy-start.1 = (bf16[256,4096]{1,0:T(8,128)(2,1)S(1)}, bf16[256,4096]{1,0:T(8,128)(2,1)}, u32[]{:S(2)}) copy-start(bf16[256,4096]{1,0:T(8,128)(2,1)} %param.28) | copy-start | bytes 6291460
Sparse Core Ops, SparseCore 0:
  56.0 33.0 reduce-scatter.2
  120.7 217.6 all-gather.2
  359.4 22.9 reduce-scatter.4
